TPU v7x, 512 devices: a whole 4x8x8 slice. The times are simulated.
512 devices in a mesh: fs: 64 (over z, y), tp: 8 (over x, core).
Axes of the slice: x: 4, y: 8, z: 8, core: 2. Of those that a mesh axis runs over, the one named last changes fastest.
Arguments:
- tokens: bfloat16 [8192, 2048], P('fs'), may hold values from -6 to 6
- norm_gain: float32 [2048], replicated, may hold values from 0.1 to 1.9
- w_query: bfloat16 [2048, 1024], P('fs', 'tp'), may hold values from -0.125 to 0.125
- w_key: bfloat16 [2048, 1024], P('fs', 'tp'), may hold values from -0.125 to 0.125
- w_value: bfloat16 [2048, 2048], P('fs', 'tp'), may hold values from -0.125 to 0.125
- w_gate: bfloat16 [2048, 2048], P('fs', 'tp'), may hold values from -0.125 to 0.125
- mixer_gain: float32 [2048], P('tp'), may hold values from 0.1 to 1.9
- w_out: bfloat16 [2048, 2048], P('tp', 'fs'), may hold values from -0.125 to 0.125
- channel_gain: float32 [2048], replicated, may hold values from 0.1 to 1.9
- w_left: bfloat16 [2048, 3072], P('fs', 'tp'), may hold values from -0.125 to 0.125
- w_right: bfloat16 [2048, 3072], P('fs', 'tp'), may hold values from -0.125 to 0.125
- taps_left: float32 [3, 3072], P(None, 'tp'), may hold values from -3.5 to 3.5
- taps_right: float32 [3, 3072], P(None, 'tp'), may hold values from -3.5 to 3.5
- w_down: bfloat16 [3072, 2048], P('tp', 'fs'), may hold values from -0.109375 to 0.109375
Outputs:
- layer_out: bfloat16 [8192, 2048], P('fs')
All inputs are finite; a program needn't handle non-finite values.
Results may differ from a plain program's by a relative error of at most 0.018.
Values may be sent and summed in bfloat16 or wider, within the bound.
No kernel may reach another device: no remote copies, remote signals or barrier semaphores. Data moves between devices by JAX's collectives and lax.ppermute only.
A program may use at most 64 MiB of HBM per device.

v0:
```python
import jax
import jax.numpy as jnp
from jax import lax
from jax.sharding import PartitionSpec as P

DK = 128
DV = 256
BLOCK = 128


highest = lax.Precision.HIGHEST


def sent_together(arrays, axis, dim, along):
    widths = [a.shape[along] for a in arrays]
    both = jnp.concatenate(arrays, axis=along)
    out = lax.all_gather(both, axis, axis=dim, tiled=True)
    return tuple(jnp.split(out, [sum(widths[:k]) for k in range(1, len(widths))], axis=along))


def copy_for_each(x, axis):
    copies = jnp.broadcast_to(x, (lax.axis_size(axis), *x.shape))
    return lax.all_to_all(copies, axis, split_axis=0, concat_axis=0, tiled=True)


def laid_out(parts, dim):
    parts = jnp.moveaxis(parts, 0, dim)
    dims = parts.shape
    return parts.reshape(*dims[:dim], dims[dim] * dims[dim + 1], *dims[dim + 2 :])


def gathered_copies(x, axis, dim):
    parts = copy_for_each(x, axis)
    return laid_out(parts, dim)


def split_up(x, dim, peers):
    dims = x.shape
    parts = x.reshape(*dims[:dim], peers, dims[dim] // peers, *dims[dim + 1 :])
    return jnp.moveaxis(parts, dim, 0)


def sent_and_summed(x, axis, dim):
    parts = split_up(x, dim, lax.axis_size(axis))
    arrived = lax.all_to_all(parts, axis, split_axis=0, concat_axis=0, tiled=True)
    return arrived.astype(jnp.float32).sum(axis=0)


def over_copies(x, axis):
    everything = copy_for_each(x, axis)
    return jnp.sum(everything.astype(jnp.float32), axis=0)


def scale_rows(rows_in, gain_vec):
    floats = rows_in.astype(jnp.float32)
    factor = lax.rsqrt(jnp.mean(floats * floats, axis=-1, keepdims=True) + 1e-06)
    return (floats * factor * gain_vec).astype(jnp.bfloat16)


def decays(first_head, count):
    head_ids = first_head + jnp.arange(count, dtype=jnp.float32)
    return jnp.log(1.0 - 2.0 ** (-5.0 - head_ids))


def rotate(heads_in, positions):
    width = heads_in.shape[-1]
    half = width // 2
    freqs = 10000.0 ** (-jnp.arange(half, dtype=jnp.float32) / half)
    angles = positions[:, None] * freqs[None, :]
    cosine = jnp.cos(angles)
    sine = jnp.sin(angles)
    first_half = heads_in[..., :half]
    second_half = heads_in[..., half:]
    return jnp.concatenate(
        [first_half * cosine - second_half * sine, first_half * sine + second_half * cosine],
        axis=-1,
    )


def retention(queries, keys_in, values_in, log_gamma):
    head_count, length, key_width = queries.shape
    value_width = values_in.shape[-1]
    blocks = length // BLOCK
    queries = queries.reshape(head_count, blocks, BLOCK, key_width)
    keys_in = keys_in.reshape(head_count, blocks, BLOCK, key_width)
    values_in = values_in.reshape(head_count, blocks, BLOCK, value_width)
    offsets = jnp.arange(BLOCK, dtype=jnp.float32)
    distance = offsets[:, None] - offsets[None, :]
    weights = jnp.where(
        distance >= 0, jnp.exp(log_gamma[:, None, None] * jnp.maximum(distance, 0.0)), 0.0
    )
    scores = jnp.einsum("hbnd,hbmd->hbnm", queries, keys_in, precision=highest) * weights[:, None]
    inner = jnp.einsum("hbnm,hbme->hbne", scores, values_in, precision=highest)
    key_weight = jnp.exp(log_gamma[:, None] * (BLOCK - 1 - offsets)[None, :])
    contrib = jnp.einsum(
        "hbjd,hbje->hbde", keys_in * key_weight[:, None, :, None], values_in, precision=highest
    )
    block_decay = jnp.exp(log_gamma * BLOCK)[:, None, None]

    def advance(state, contrib_block):
        return (state * block_decay + contrib_block, state)

    _, states = lax.scan(
        advance,
        jnp.zeros((head_count, key_width, value_width), jnp.float32),
        jnp.moveaxis(contrib, 1, 0),
    )
    states = jnp.moveaxis(states, 0, 1)
    query_weight = jnp.exp(log_gamma[:, None] * (offsets + 1.0)[None, :])
    carried = (
        jnp.einsum("hbnd,hbde->hbne", queries, states, precision=highest)
        * query_weight[:, None, :, None]
    )
    return (inner + carried).reshape(head_count, length, value_width)


def head_norm(retained):
    return retained * lax.rsqrt(jnp.mean(retained * retained, axis=-1, keepdims=True) + 1e-06)


def causal_taps(values_in, taps):
    length = values_in.shape[-2]
    padded = jnp.pad(values_in.astype(jnp.float32), ((taps.shape[0] - 1, 0), (0, 0)))
    result = padded[0:length] * taps[0]
    for tap_index in range(1, taps.shape[0]):
        result = result + padded[tap_index : tap_index + length] * taps[tap_index]
    return result


def fold_tuple(source, pieces):
    return tuple(
        (
            jnp.dot(source, weight_piece, preferred_element_type=jnp.float32)
            for weight_piece in pieces
        )
    )


def body(
    tokens,
    norm_gain,
    w_query,
    w_key,
    w_value,
    w_gate,
    mixer_gain,
    w_out,
    channel_gain,
    w_left,
    w_right,
    taps_left,
    taps_right,
    w_down,
):
    length = tokens.shape[0]
    normed = scale_rows(tokens, norm_gain)
    queries, keys_proj, values_proj, gates = fold_tuple(
        normed, sent_together((w_query, w_key, w_value, w_gate), "fs", 0, 1)
    )
    queries = queries.astype(jnp.bfloat16)
    keys_proj = keys_proj.astype(jnp.bfloat16)
    values_proj = values_proj.astype(jnp.bfloat16)
    gates = gates.astype(jnp.bfloat16)
    heads_here = w_query.shape[1] // DK
    first_head = (lax.axis_index("tp") * heads_here).astype(jnp.float32)
    log_gamma = decays(first_head, heads_here)
    positions = jnp.arange(length, dtype=jnp.float32)

    def split_heads(rows_in, width):
        return rows_in.astype(jnp.float32).reshape(length, heads_here, width).transpose(1, 0, 2)

    retained = head_norm(
        retention(
            rotate(split_heads(queries, DK), positions),
            rotate(split_heads(keys_proj, DK), positions),
            split_heads(values_proj, DV),
            log_gamma,
        )
    )
    retained = retained.transpose(1, 0, 2).reshape(length, heads_here * DV)
    hidden = (retained * mixer_gain * jax.nn.silu(gates.astype(jnp.float32))).astype(jnp.bfloat16)
    rows_own = length // lax.axis_size("tp")
    first_row = lax.axis_index("tp") * rows_own
    out_whole = gathered_copies(w_out, "fs", 1)
    mixer_total = sent_and_summed(
        jnp.dot(hidden, out_whole, preferred_element_type=jnp.float32).astype(jnp.bfloat16), "tp", 0
    )
    residual = lax.dynamic_slice_in_dim(tokens, first_row, rows_own, 0)
    middle_own = (residual.astype(jnp.float32) + mixer_total).astype(jnp.bfloat16)
    middle = gathered_copies(middle_own, "tp", 0)
    normed_mid = scale_rows(middle, channel_gain)
    left, right = fold_tuple(normed_mid, sent_together((w_left, w_right), "fs", 0, 1))
    left = left.astype(jnp.bfloat16)
    right = right.astype(jnp.bfloat16)
    gated = (jax.nn.silu(causal_taps(left, taps_left)) * causal_taps(right, taps_right)).astype(
        jnp.bfloat16
    )
    down_whole = lax.all_gather(w_down, "fs", axis=1, tiled=True)
    channel_part = jnp.dot(gated, down_whole, preferred_element_type=jnp.float32)
    channel_total = over_copies(channel_part.astype(jnp.bfloat16), "tp").astype(jnp.float32)
    return (middle.astype(jnp.float32) + channel_total).astype(jnp.bfloat16)


def solution(mesh):
    placed = (
        P("fs", None),
        P(),
        P("fs", "tp"),
        P("fs", "tp"),
        P("fs", "tp"),
        P("fs", "tp"),
        P("tp"),
        P("tp", "fs"),
        P(),
        P("fs", "tp"),
        P("fs", "tp"),
        P(None, "tp"),
        P(None, "tp"),
        P("tp", "fs"),
    )
    return jax.shard_map(body, mesh=mesh, in_specs=placed, out_specs=P("fs", None), check_vma=False)
```

profile of v0, /device:TPU:1, one launch (start us, length us, event | category | flops | bytes accessed | tf_op | source)
XLA Modules:
  0.0 344.2 jit_solution(9622358227340989568)
XLA Ops:
  6.5 1.4 pad_maximum_fusion
  8.0 1.4 pad_maximum_fusion.1
  9.4 1.9 broadcast_in_dim.13
  11.4 17.1 %all-to-all-start = ((bf16[64,256,32]{1,2,0:T(8,128)(2,1)}), bf16[64,256,32]{1,2,0:T(8,128)(2,1)S(1)}, u32[]{:S(2)}, u32[]{:S(2)}) async-start(bf16[64,256,32]{1,2,0:T(8,128)(2,1)} %broadcast_in_dim.13), calls=%async_computation | async-start | bytes 2097152 | tf_op jit(solution)/shard_map/all_to_all | solution.py:23
  28.5 0.7 all-gather.8.cloned.1.call-update
  29.3 0.2 fusion.21
  29.6 79.5 %all-gather.4.cloned.1.call-done = bf16[2048,768]{1,0:T(8,128)(2,1)} async-done(((bf16[32,768]{1,0:T(8,128)(2,1)}), bf16[2048,768]{1,0:T(8,128)(2,1)}) %all-gather.4.cloned.1.call-update) | async-done | bytes 3145744 | tf_op jit(solution)/shard_map/all_gather | solution.py:17
  109.1 1.4 fusion.18
  110.6 1.4 fusion.20
  112.0 0.2 multiply_subtract_fusion
  112.2 0.3 convolution_multiply_fusion.1
  112.5 0.3 convolution_multiply_fusion
  112.8 1.6 convolution_convert_fusion.3
  114.4 0.3 multiply_reduce_fusion
  114.7 3.0 convolution_convert_fusion.1
  117.7 8.6 %all-to-all-start.1 = ((bf16[8,16,2048]{2,1,0:T(8,128)(2,1)}), bf16[8,16,2048]{2,1,0:T(8,128)(2,1)S(1)}, u32[]{:S(2)}, u32[]{:S(2)}) async-start(bf16[8,16,2048]{2,1,0:T(8,128)(2,1)} %bitcast.8), calls=%async_computation.1 | async-start | bytes 1048576 | tf_op jit(solution)/shard_map/all_to_all | solution.py:45
  126.3 9.3 %all-to-all-done.1 = bf16[8,16,2048]{2,1,0:T(8,128)(2,1)S(1)} async-done(((bf16[8,16,2048]{2,1,0:T(8,128)(2,1)}), bf16[8,16,2048]{2,1,0:T(8,128)(2,1)S(1)}, u32[]{:S(2)}, u32[]{:S(2)}) %all-to-all-start.1) | async-done | bytes 524320 | tf_op jit(solution)/shard_map/all_to_all | solution.py:45
  135.8 0.8 broadcast_in_dim.14
  136.6 4.4 %all-to-all-start.2 = ((bf16[8,16,2048]{2,1,0:T(8,128)(2,1)}), bf16[8,16,2048]{2,1,0:T(8,128)(2,1)S(1)}, u32[]{:S(2)}, u32[]{:S(2)}) async-start(bf16[8,16,2048]{2,1,0:T(8,128)(2,1)} %broadcast_in_dim.14), calls=%async_computation.2 | async-start | bytes 1048576 | tf_op jit(solution)/shard_map/all_to_all | solution.py:23
  141.0 9.3 %all-to-all-done.2 = bf16[8,16,2048]{2,1,0:T(8,128)(2,1)S(1)} async-done(((bf16[8,16,2048]{2,1,0:T(8,128)(2,1)}), bf16[8,16,2048]{2,1,0:T(8,128)(2,1)S(1)}, u32[]{:S(2)}, u32[]{:S(2)}) %all-to-all-start.2) | async-done | bytes 524320 | tf_op jit(solution)/shard_map/all_to_all | solution.py:23
  150.4 0.2 fusion.26
  150.5 0.1 rsqrt.30
  150.6 0.2 fusion.28
  150.8 43.1 %all-gather.6.cloned.1.call-done = bf16[2048,768]{1,0:T(8,128)(2,1)} async-done(((bf16[32,768]{1,0:T(8,128)(2,1)}), bf16[2048,768]{1,0:T(8,128)(2,1)}) %all-gather.6.cloned.1.call-update) | async-done | bytes 3145744 | tf_op jit(solution)/shard_map/all_gather | solution.py:17
  193.9 1.9 fusion.13
  195.8 1.9 fusion.7
  197.6 78.1 %all-gather.8.cloned.1.call-done = bf16[384,2048]{0,1:T(8,128)(2,1)} async-done(((bf16[384,32]{0,1:T(8,128)(2,1)}), bf16[384,2048]{0,1:T(8,128)(2,1)}) %all-gather.8.cloned.1.call-update) | async-done | bytes 1572880 | tf_op jit(solution)/shard_map/all_gather | solution.py:198
  275.7 2.1 convolution_convert_fusion
  277.8 0.5 broadcast_in_dim.15
  278.4 57.7 %all_to_all.20 = bf16[8,128,2048]{2,1,0:T(8,128)(2,1)S(1)} all-to-all(bf16[8,128,2048]{2,1,0:T(8,128)(2,1)S(1)} %broadcast_in_dim.15), channel_id=1, replica_groups=mesh['fs'=64,'tp'=8] {'tp'}, dimensions={0} | all-to-all | bytes 8388608 | tf_op jit(solution)/shard_map/all_to_all | solution.py:23
  336.0 0.7 convert_reduce_fusion
  336.7 0.9 fusion.29
  (26 shorter events, 0.3 us)
Async XLA Ops:
  6.5 22.7 %copy-start = (bf16[128,2048]{1,0:T(8,128)(2,1)S(1)}, bf16[128,2048]{1,0:T(8,128)(2,1)}, u32[]{:S(2)}) copy-start(bf16[128,2048]{1,0:T(8,128)(2,1)} %param.14) | copy-start | bytes 1572868
  6.5 102.6 %copy-start.4 = (f32[2048]{0:T(1024)S(1)}, f32[2048]{0:T(1024)}, u32[]{:S(2)}) copy-start(f32[2048]{0:T(1024)} %param.15) | copy-start | bytes 24580
  6.5 102.6 %all-gather.4.cloned.1.call-start = ((), (), s32[]{:S(2)}) async-start(), calls=%async_computation.4 | async-start | bytes 3194880 | tf_op jit(solution)/shard_map/all_gather | solution.py:17
  8.0 185.9 %all-gather.6.cloned.1.call-start = ((), (), s32[]{:S(2)}) async-start(), calls=%async_computation.5 | async-start | bytes 3194880 | tf_op jit(solution)/shard_map/all_gather | solution.py:17
  11.4 103.3 %all-to-all-start = ((bf16[64,256,32]{1,2,0:T(8,128)(2,1)}), bf16[64,256,32]{1,2,0:T(8,128)(2,1)S(1)}, u32[]{:S(2)}, u32[]{:S(2)}) async-start(bf16[64,256,32]{1,2,0:T(8,128)(2,1)} %broadcast_in_dim.13), calls=%async_computation | async-start | bytes 2097152 | tf_op jit(solution)/shard_map/all_to_all | solution.py:23
  28.5 247.2 %all-gather.8.cloned.1.call-start = ((), (), s32[]{:S(2)}) async-start(), calls=%async_computation.6 | async-start | bytes 1597440 | tf_op jit(solution)/shard_map/all_gather | solution.py:198
  29.6 85.1 %copy-start.5 = (f32[256]{0:T(256)S(1)}, f32[256]{0:T(256)}, u32[]{:S(2)}) copy-start(f32[256]{0:T(256)} %param.20) | copy-start | bytes 3076
  114.7 26.3 %copy-start.2 = (f32[3,384]{1,0:T(4,128)S(1)}, f32[3,384]{1,0:T(4,128)}, u32[]{:S(2)}) copy-start(f32[3,384]{1,0:T(4,128)} %param.26) | copy-start | bytes 13828
  114.7 26.3 %copy-start.3 = (f32[3,384]{1,0:T(4,128)S(1)}, f32[3,384]{1,0:T(4,128)}, u32[]{:S(2)}) copy-start(f32[3,384]{1,0:T(4,128)} %param.25) | copy-start | bytes 13828
  114.7 35.9 %copy-start.1 = (f32[2048]{0:T(1024)S(1)}, f32[2048]{0:T(1024)}, u32[]{:S(2)}) copy-start(f32[2048]{0:T(1024)} %param.22) | copy-start | bytes 24580
  117.7 17.9 %all-to-all-start.1 = ((bf16[8,16,2048]{2,1,0:T(8,128)(2,1)}), bf16[8,16,2048]{2,1,0:T(8,128)(2,1)S(1)}, u32[]{:S(2)}, u32[]{:S(2)}) async-start(bf16[8,16,2048]{2,1,0:T(8,128)(2,1)} %bitcast.8), calls=%async_computation.1 | async-start | bytes 1048576 | tf_op jit(solution)/shard_map/all_to_all | solution.py:45
  136.6 13.7 %all-to-all-start.2 = ((bf16[8,16,2048]{2,1,0:T(8,128)(2,1)}), bf16[8,16,2048]{2,1,0:T(8,128)(2,1)S(1)}, u32[]{:S(2)}, u32[]{:S(2)}) async-start(bf16[8,16,2048]{2,1,0:T(8,128)(2,1)} %broadcast_in_dim.14), calls=%async_computation.2 | async-start | bytes 1048576 | tf_op jit(solution)/shard_map/all_to_all | solution.py:23
Sparse Core Ops, SparseCore 0:
  10.3 98.7 all-gather.3
  112.1 81.7 all-gather.5
  196.9 78.7 all-gather.7
where the time goes:
time: 345 us; the launch traced here: 344 us
  waiting for transfers between devices  220 us (64%)
  blocking collectives  57.7 us (17%)
  starting transfers between devices  30.1 us (9%)
  matrix products  14.1 us (4%)
  between operations  13.4 us (4%)
  other arithmetic  5.32 us (2%)
  local copies, waits for them, and re-layouts  3.45 us (1%)
    all_gather x2, waiting for transfers between devices, sent_together(): out = lax.all_gather(both, axis, axis=dim, tiled=True)  123 us
    all_gather x1, waiting for transfers between devices, body(): down_whole = lax.all_gather(w_down, 'fs', axis=1, tiled=True)  78.1 us
    all_to_all x1, blocking collectives, copy_for_each(): return lax.all_to_all(copies, axis, split_axis=0, concat_axis=0, tiled=True)  57.7 us
    all_to_all x2, starting transfers between devices, copy_for_each(): return lax.all_to_all(copies, axis, split_axis=0, concat_axis=0, tiled=True)  21.5 us
    all_to_all x1, waiting for transfers between devices, sent_and_summed(): lax.all_to_all(parts, axis, split_axis=0, concat_axis=0, tiled=True)  9.35 us
    all_to_all x2, waiting for transfers between devices, copy_for_each(): return lax.all_to_all(copies, axis, split_axis=0, concat_axis=0, tiled=True)  9.33 us
    all_to_all x1, starting transfers between devices, sent_and_summed(): lax.all_to_all(parts, axis, split_axis=0, concat_axis=0, tiled=True)  8.57 us
    dot_general x5, matrix products, fold_tuple(): jnp.dot(source, weight_piece, preferred_element_type=jnp.float32)  8.17 us
  transfers between devices with their start and end apart: 6, of which 5 were waited for; matrix products, arithmetic and copies ran while one was open for 5% of the time, Pallas kernels for 0%

commit v1 on v0

v1 whole, which is shorter than its diff:
```python
import functools

import jax
import jax.numpy as jnp
from jax import lax
from jax.experimental import pallas as pl
from jax.experimental.pallas import tpu as pltpu
from jax.sharding import Mesh
from jax.sharding import PartitionSpec as P

DK = 128
DV = 256
FIRST_ROWS = 16
FS = ("zh", "zl", "yh", "yl")
FAR = ("zh", "yh")
NEAR = ("zl", "yl")
TP = ("x", "c")
highest = lax.Precision.HIGHEST


def size_of(axes):
    axes = (axes,) if isinstance(axes, str) else axes
    total = 1
    for name in axes:
        total *= lax.axis_size(name)
    return total


def swap(parts, axes):
    return lax.all_to_all(parts, axes, split_axis=0, concat_axis=0, tiled=True)


def copies_from(x, axes):
    return swap(jnp.broadcast_to(x, (size_of(axes), *x.shape)), axes)


def pack_body(early_count, *refs):
    ins, (early_ref, late_ref) = refs[:-2], refs[-2:]
    early = jnp.concatenate([ref[...] for ref in ins[:early_count]], axis=1)
    for i in range(early_ref.shape[0]):
        early_ref[i] = early
    late_ref[...] = jnp.concatenate([ref[...] for ref in ins[early_count:]], axis=1)


def pack(copies, early, late):
    arrays = [*early, *late]
    rows = arrays[0].shape[0]
    whole = pl.BlockSpec(memory_space=pltpu.VMEM)
    shapes = [
        (copies, rows, sum(a.shape[1] for a in early)),
        (rows, sum(a.shape[1] for a in late)),
    ]
    return pl.pallas_call(
        functools.partial(pack_body, len(early)),
        out_shape=[jax.ShapeDtypeStruct(shape, jnp.bfloat16) for shape in shapes],
        in_specs=[whole] * len(arrays),
        out_specs=[whole] * len(shapes),
    )(*arrays)


def scale_rows(rows_in, gain_vec):
    floats = rows_in.astype(jnp.float32)
    factor = lax.rsqrt(jnp.mean(floats * floats, axis=-1, keepdims=True) + 1e-06)
    return (floats * factor * gain_vec).astype(jnp.bfloat16)


def rotate(rows_in, positions):
    half = rows_in.shape[-1] // 2
    freqs = 10000.0 ** (-jnp.arange(half, dtype=jnp.float32) / half)
    angles = positions[:, None] * freqs[None, :]
    cosine = jnp.cos(angles)
    sine = jnp.sin(angles)
    first_half = rows_in[:, :half]
    second_half = rows_in[:, half:]
    return jnp.concatenate(
        [first_half * cosine - second_half * sine, first_half * sine + second_half * cosine],
        axis=-1,
    )


def retention(queries, keys_in, values_in, log_gamma):
    offsets = jnp.arange(queries.shape[0], dtype=jnp.float32)
    distance = offsets[:, None] - offsets[None, :]
    weights = jnp.where(distance >= 0, jnp.exp(log_gamma * jnp.maximum(distance, 0.0)), 0.0)
    scores = jnp.einsum("nd,md->nm", queries, keys_in, precision=highest) * weights
    return jnp.einsum("nm,me->ne", scores, values_in, precision=highest)


def causal_taps(values_in, taps):
    length = values_in.shape[-2]
    padded = jnp.pad(values_in.astype(jnp.float32), ((taps.shape[0] - 1, 0), (0, 0)))
    result = padded[0:length] * taps[0]
    for tap_index in range(1, taps.shape[0]):
        result = result + padded[tap_index : tap_index + length] * taps[tap_index]
    return result


def dot32(a, b):
    return jnp.dot(a, b, preferred_element_type=jnp.float32)


def near_parts(rows_in):
    rows = rows_in.shape[0]
    far_z, near_z, far_y, near_y = (lax.axis_size(a) for a in FS)
    width = rows_in.shape[1] // (far_z * near_z * far_y * near_y)
    parts = rows_in.reshape(rows, far_z, near_z, far_y, near_y, width)
    parts = parts.transpose(2, 4, 0, 1, 3, 5)
    return parts.reshape(near_z * near_y, rows, far_z * far_y * width)


def from_near_parts(parts):
    far_z, near_z, far_y, near_y = (lax.axis_size(a) for a in FS)
    rows = parts.shape[1]
    width = parts.shape[2] // (far_z * far_y)
    parts = parts.reshape(near_z, near_y, rows, far_z, far_y, width)
    return parts.transpose(2, 3, 0, 4, 1, 5).reshape(rows, -1)


def body(
    tokens,
    norm_gain,
    w_query,
    w_key,
    w_value,
    w_gate,
    mixer_gain,
    w_out,
    channel_gain,
    w_left,
    w_right,
    taps_left,
    taps_right,
    w_down,
):
    length, width = tokens.shape
    near = size_of(NEAR)
    far = size_of(FAR)
    peers = size_of(TP)
    units = w_left.shape[1]

    first, second = pack(
        far, (w_query, w_key, w_value, w_gate, w_out.T), (w_left, w_right, w_down.T)
    )
    late = lax.all_gather(second, FS, axis=0, tiled=True)
    early = swap(first, ("yh", "zh")).reshape(4, 4, w_left.shape[0], -1)
    early = early.transpose(1, 0, 2, 3).reshape(width // near, -1)
    proj_cols = early.shape[1] - DV

    normed = near_parts(scale_rows(tokens, norm_gain))
    me = lax.axis_index(NEAR)
    held = jnp.zeros((near, length, width // near), jnp.bfloat16)
    for d in range(near):
        piece = lax.dynamic_index_in_dim(normed, me ^ d, 0, keepdims=True)
        if d:
            piece = lax.ppermute(piece, NEAR, [(i, i ^ d) for i in range(near)])
        held = lax.dynamic_update_slice_in_dim(held, piece, me ^ d, 0)
    held = held.reshape(near * length, -1)
    part = dot32(held, early[:, :proj_cols]).reshape(near, length, proj_cols)
    fine_part = part[:, :FIRST_ROWS, : 2 * DK]
    fine_part = fine_part - lax.reduce_precision(fine_part, 8, 7)
    middle_bits = lax.reduce_precision(fine_part, 8, 7)
    extra = [middle_bits, fine_part - middle_bits]
    extra.append(jnp.zeros((near, FIRST_ROWS, proj_cols - 4 * DK), jnp.float32))
    part = jnp.concatenate([part, jnp.concatenate(extra, axis=2)], axis=1).astype(jnp.bfloat16)
    part = swap(part, NEAR).astype(jnp.float32)
    total = part[0]
    for d in range(1, near):
        total = total + part[d]
    extra = total[length:, : 2 * DK] + total[length:, 2 * DK : 4 * DK]
    total = total[:length] + jnp.pad(
        extra, ((0, length - FIRST_ROWS), (0, proj_cols - 2 * DK))
    )
    total = lax.reduce_precision(total, 8, 7)
    queries, keys_proj = total[:, :DK], total[:, DK : 2 * DK]
    values_proj, gates = total[:, 2 * DK : 2 * DK + DV], total[:, 2 * DK + DV :]

    head = lax.axis_index(TP).astype(jnp.float32)
    log_gamma = jnp.log(1.0 - 2.0 ** (-5.0 - head))
    positions = jnp.arange(length, dtype=jnp.float32)
    retained = retention(
        rotate(queries, positions), rotate(keys_proj, positions), values_proj, log_gamma
    )
    retained = retained * lax.rsqrt(jnp.mean(retained * retained, axis=-1, keepdims=True) + 1e-06)
    hidden = (retained * mixer_gain * jax.nn.silu(gates)).astype(jnp.bfloat16)

    rows_own = length // peers
    first_row = lax.axis_index(TP) * rows_own
    hidden_near = copies_from(hidden, NEAR).reshape(near * length, DV)
    mixed = lax.dot_general(
        hidden_near,
        early[:, proj_cols:],
        (((1,), (1,)), ((), ())),
        preferred_element_type=jnp.float32,
    ).astype(jnp.bfloat16)
    mixed = mixed.reshape(near * peers // 2, 2, rows_own, -1)
    core = lax.axis_index("c")
    kept = lax.dynamic_index_in_dim(mixed, core, 1, keepdims=False).astype(jnp.float32)
    given = lax.dynamic_index_in_dim(mixed, 1 - core, 1, keepdims=False)
    taken = lax.ppermute(given, "c", [(0, 1), (1, 0)]).astype(jnp.float32)
    arrived = swap((kept + taken).astype(jnp.bfloat16), (*NEAR, "x")).astype(jnp.float32)
    arrived = arrived.reshape(near, peers // 2, rows_own, -1).sum(axis=1)
    residual = lax.dynamic_slice_in_dim(tokens, first_row, rows_own, 0)
    middle_own = (residual.astype(jnp.float32) + from_near_parts(arrived)).astype(jnp.bfloat16)
    normed_mid = lax.all_gather(scale_rows(middle_own, channel_gain), TP, axis=0, tiled=True)

    both = dot32(normed_mid, late[:, : 2 * units]).astype(jnp.bfloat16)
    left, right = both[:, :units], both[:, units:]
    gated = (jax.nn.silu(causal_taps(left, taps_left)) * causal_taps(right, taps_right)).astype(
        jnp.bfloat16
    )
    channel_part = lax.dot_general(
        gated, late[:, 2 * units :], (((1,), (1,)), ((), ())), preferred_element_type=jnp.float32
    ).astype(jnp.bfloat16)
    channel = swap(channel_part.reshape(peers, rows_own, width), TP)
    channel = channel.astype(jnp.float32).sum(axis=0)
    own = (middle_own.astype(jnp.float32) + channel).astype(jnp.bfloat16)
    return lax.all_gather(own, TP, axis=0, tiled=True)


def solution(mesh):
    fs, tp = mesh.devices.shape
    fine = Mesh(mesh.devices.reshape(4, 2, 4, fs // 32, tp // 2, 2), (*FS, *TP))
    placed = (
        P(FS, None),
        P(),
        P(FS, TP),
        P(FS, TP),
        P(FS, TP),
        P(FS, TP),
        P(TP),
        P(TP, FS),
        P(),
        P(FS, TP),
        P(FS, TP),
        P(None, TP),
        P(None, TP),
        P(TP, FS),
    )
    return jax.shard_map(body, mesh=fine, in_specs=placed, out_specs=P(FS, None), check_vma=False)
```

time: 345 us -> 165 us (0.48)
  waiting for transfers between devices: 220 us -> 52.2 us
  blocking collectives: 57.7 us -> 40.7 us
  starting transfers between devices: 30.1 us -> 41.6 us
  matrix products: 14.1 us -> 6.18 us
    all_gather x3 -> x1, waiting for transfers between devices: 201 us -> 0.01 us  [body(): late = lax.all_gather(second, FS, axis=0, tiled=True)]
    all_to_all x1, blocking collectives: 57.7 us -> 12 us  [swap(): return lax.all_to_all(parts, axes, split_axis=0, concat_axis=0, tiled=True)]
    all_gather x0 -> x2, blocking collectives: none -> 28.7 us  [the longest x1 14.7 us: body(): lax.all_gather(scale_rows(middle_own, channel_gain), TP, axis=0, tiled=True)]
    ppermute x0 -> x4, waiting for transfers between devices: none -> 25 us  [the longest x3 23.9 us: body(): piece = lax.ppermute(piece, NEAR, [(i, i ^ d) for i in range(near)])]
    ppermute x0 -> x4, starting transfers between devices: none -> 13.3 us  [the longest x3 8.37 us: body(): piece = lax.ppermute(piece, NEAR, [(i, i ^ d) for i in range(near)])]
    all_to_all x3 -> x4, waiting for transfers between devices: 18.7 us -> 27.2 us  [swap(): return lax.all_to_all(parts, axes, split_axis=0, concat_axis=0, tiled=True)]
    dot_general x10 -> x6, matrix products: 14.1 us -> 6.18 us  [the longest x2 3.05 us: dot32(): return jnp.dot(a, b, preferred_element_type=jnp.float32)]
    all_to_all x3 -> x4, starting transfers between devices: 30.1 us -> 28.3 us  [swap(): return lax.all_to_all(parts, axes, split_axis=0, concat_axis=0, tiled=True)]
  transfers between devices with their start and end apart: 6 -> 9, of which waited for: 5 -> 7; matrix products, arithmetic and copies ran while one was open for 5% -> 5% of each run, Pallas kernels for 0% -> 0%
where the time goes in v1:
time: 165 us; the launch traced here: 164 us
  waiting for transfers between devices  52.2 us (32%)
  starting transfers between devices  41.6 us (25%)
  blocking collectives  40.7 us (25%)
  between operations  13.9 us (8%)
  matrix products  6.18 us (4%)
  local copies, waits for them, and re-layouts  3.97 us (2%)
  other arithmetic  3.7 us (2%)
  Pallas kernels  2.07 us (1%)
    all_to_all x4, starting transfers between devices, swap(): return lax.all_to_all(parts, axes, split_axis=0, concat_axis=0, tiled=True)  28.3 us
    all_to_all x4, waiting for transfers between devices, swap(): return lax.all_to_all(parts, axes, split_axis=0, concat_axis=0, tiled=True)  27.2 us
    ppermute x3, waiting for transfers between devices, body(): piece = lax.ppermute(piece, NEAR, [(i, i ^ d) for i in range(near)])  23.9 us
    all_gather x1, blocking collectives, body(): lax.all_gather(scale_rows(middle_own, channel_gain), TP, axis=0, tiled=True)  14.7 us
    all_gather x1, blocking collectives, body(): return lax.all_gather(own, TP, axis=0, tiled=True)  14 us
    all_to_all x1, blocking collectives, swap(): return lax.all_to_all(parts, axes, split_axis=0, concat_axis=0, tiled=True)  12 us
    ppermute x3, starting transfers between devices, body(): piece = lax.ppermute(piece, NEAR, [(i, i ^ d) for i in range(near)])  8.37 us
    ppermute x1, starting transfers between devices, body(): taken = lax.ppermute(given, 'c', [(0, 1), (1, 0)]).astype(jnp.float32)  4.94 us
  transfers between devices with their start and end apart: 9, of which 7 were waited for; matrix products, arithmetic and copies ran while one was open for 5% of the time, Pallas kernels for 0%

profile of v1, /device:TPU:1, one launch (start us, length us, event | category | flops | bytes accessed | tf_op | source)
XLA Modules:
  0.0 164.3 jit_solution(2401874990642138415)
XLA Ops:
  6.5 2.1 %shard_map.136 = (bf16[16,32,1024]{2,1,0:T(8,128)(2,1)}, bf16[32,1152]{1,0:T(8,128)(2,1)}) custom-call(bf16[32,128]{1,0:T(8,128)(2,1)} %refs_0_.1, bf16[32,128]{1,0:T(8,128)(2,1)} %refs_1_.1, bf16[32,256]{1,0:T(8,128)(2,1)} %refs_2_.1, bf16[32,256]{1,0:T(8,128)(2,1)} %refs_3_.1, bf16[32,256]{1,0:T(8,128)(2,1)} %bitcast.50, bf16[32,384]{1,0:T(8,128)(2,1)} %refs_5_.1, ...), custom_call_target="tpu_custom_call" | custom-call | tf_op jit(solution)/shard_map/pallas_call | solution.py:53
  8.6 16.2 %all-to-all-start = ((bf16[16,32,1024]{2,1,0:T(8,128)(2,1)}), bf16[16,32,1024]{2,1,0:T(8,128)(2,1)S(1)}, u32[]{:S(2)}, u32[]{:S(2)}) async-start(bf16[16,32,1024]{2,1,0:T(8,128)(2,1)} %get-tuple-element.7), calls=%async_computation | async-start | bytes 2097152 | tf_op jit(solution)/shard_map/all_to_all | solution.py:30
  25.5 0.3 fusion.8
  26.0 2.3 %collective-permute-start = (bf16[1,128,512]{1,2,0:T(8,128)(2,1)S(1)}, bf16[1,128,512]{1,2,0:T(8,128)(2,1)S(1)}, u32[]{:S(2)}, u32[]{:S(2)}) collective-permute-start(bf16[1,128,512]{1,2,0:T(8,128)(2,1)S(1)} %get-tuple-element.21), channel_id=1, source_target_pairs={{0,8},{8,0},{64,72},{72,64},{1,9},{9,1},{65,73},{73,65},{2,10},{10... | collective-permute-start | bytes 393224 | tf_op jit(solution)/shard_map/ppermute | solution.py:155
  28.3 3.1 %collective-permute-start.1 = (bf16[1,128,512]{1,2,0:T(8,128)(2,1)S(1)}, bf16[1,128,512]{1,2,0:T(8,128)(2,1)S(1)}, u32[]{:S(2)}, u32[]{:S(2)}) collective-permute-start(bf16[1,128,512]{1,2,0:T(8,128)(2,1)S(1)} %get-tuple-element.20), channel_id=1, source_target_pairs={{0,64},{8,72},{64,0},{72,8},{1,65},{9,73},{65,1},{73,9},{2,66},{10... | collective-permute-start | bytes 393224 | tf_op jit(solution)/shard_map/ppermute | solution.py:155
  31.4 3.0 %collective-permute-start.2 = (bf16[1,128,512]{1,2,0:T(8,128)(2,1)S(1)}, bf16[1,128,512]{1,2,0:T(8,128)(2,1)S(1)}, u32[]{:S(2)}, u32[]{:S(2)}) collective-permute-start(bf16[1,128,512]{1,2,0:T(8,128)(2,1)S(1)} %get-tuple-element.19), channel_id=1, source_target_pairs={{0,72},{8,64},{64,8},{72,0},{1,73},{9,65},{65,9},{73,1},{2,74},{10... | collective-permute-start | bytes 393224 | tf_op jit(solution)/shard_map/ppermute | solution.py:155
  34.6 14.6 %collective-permute-done = bf16[1,128,512]{1,2,0:T(8,128)(2,1)S(1)} collective-permute-done((bf16[1,128,512]{1,2,0:T(8,128)(2,1)S(1)}, bf16[1,128,512]{1,2,0:T(8,128)(2,1)S(1)}, u32[]{:S(2)}, u32[]{:S(2)}) %collective-permute-start) | collective-permute-done | bytes 131104 | tf_op jit(solution)/shard_map/ppermute | solution.py:155
  49.5 9.2 %collective-permute-done.2 = bf16[1,128,512]{1,2,0:T(8,128)(2,1)S(1)} collective-permute-done((bf16[1,128,512]{1,2,0:T(8,128)(2,1)S(1)}, bf16[1,128,512]{1,2,0:T(8,128)(2,1)S(1)}, u32[]{:S(2)}, u32[]{:S(2)}) %collective-permute-start.2) | collective-permute-done | bytes 131104 | tf_op jit(solution)/shard_map/ppermute | solution.py:155
  58.9 0.7 all-to-all-done
  59.7 0.6 fusion.51
  60.3 1.1 maximum_maximum_fusion
  61.4 3.5 %all-to-all-start.1 = ((bf16[4,144,768]{2,1,0:T(8,128)(2,1)}), bf16[4,144,768]{2,1,0:T(8,128)(2,1)S(1)}, u32[]{:S(2)}, u32[]{:S(2)}) async-start(bf16[4,144,768]{2,1,0:T(8,128)(2,1)} %maximum_maximum_fusion), calls=%async_computation.1 | async-start | bytes 1769472 | tf_op jit(solution)/shard_map/all_to_all | solution.py:30
  65.0 11.4 %all-to-all-done.1 = bf16[4,144,768]{2,1,0:T(8,128)(2,1)S(1)} async-done(((bf16[4,144,768]{2,1,0:T(8,128)(2,1)}), bf16[4,144,768]{2,1,0:T(8,128)(2,1)S(1)}, u32[]{:S(2)}, u32[]{:S(2)}) %all-to-all-start.1) | async-done | bytes 884768 | tf_op jit(solution)/shard_map/all_to_all | solution.py:30
  77.2 0.3 convolution_multiply_fusion
  77.5 0.3 multiply_reduce_fusion
  78.0 0.7 broadcast_in_dim.9
  78.7 3.5 %all-to-all-start.2 = ((bf16[4,128,256]{2,1,0:T(8,128)(2,1)}), bf16[4,128,256]{2,1,0:T(8,128)(2,1)S(1)}, u32[]{:S(2)}, u32[]{:S(2)}) async-start(bf16[4,128,256]{2,1,0:T(8,128)(2,1)} %broadcast_in_dim.9), calls=%async_computation.2 | async-start | bytes 524288 | tf_op jit(solution)/shard_map/all_to_all | solution.py:30
  82.3 4.2 %all-to-all-done.2 = bf16[4,128,256]{2,1,0:T(8,128)(2,1)S(1)} async-done(((bf16[4,128,256]{2,1,0:T(8,128)(2,1)}), bf16[4,128,256]{2,1,0:T(8,128)(2,1)S(1)}, u32[]{:S(2)}, u32[]{:S(2)}) %all-to-all-start.2) | async-done | bytes 262176 | tf_op jit(solution)/shard_map/all_to_all | solution.py:30
  86.4 0.3 convolution_convert_fusion.1
  86.8 4.9 %collective-permute-start.3 = (bf16[16,16,512]{2,1,0:T(8,128)(2,1)S(1)}, bf16[16,16,512]{2,1,0:T(8,128)(2,1)S(1)}, u32[]{:S(2)}, u32[]{:S(2)}) collective-permute-start(bf16[16,16,512]{2,1,0:T(8,128)(2,1)S(1)} %dynamic-slice_bitcast_fusion), channel_id=1, source_target_pairs={{0,1},{1,0},{2,3},{3,2},{4,5},{5,4},{6,7},{7,6},{8,9},{9,8},{10,11... | collective-permute-start | bytes 786440 | tf_op jit(solution)/shard_map/ppermute | solution.py:199
  91.8 1.1 collective-permute-done.3
  92.9 0.8 fusion.10
  93.7 5.0 %all-to-all-start.3 = ((bf16[16,16,512]{2,1,0:T(8,128)(2,1)}), bf16[16,16,512]{2,1,0:T(8,128)(2,1)S(1)}, u32[]{:S(2)}, u32[]{:S(2)}) async-start(bf16[16,16,512]{2,1,0:T(8,128)(2,1)} %fusion.10), calls=%async_computation.3 | async-start | bytes 524288 | tf_op jit(solution)/shard_map/all_to_all | solution.py:30
  98.8 10.8 %all-to-all-done.3 = bf16[16,16,512]{2,1,0:T(8,128)(2,1)S(1)} async-done(((bf16[16,16,512]{2,1,0:T(8,128)(2,1)}), bf16[16,16,512]{2,1,0:T(8,128)(2,1)S(1)}, u32[]{:S(2)}, u32[]{:S(2)}) %all-to-all-start.3) | async-done | bytes 262176 | tf_op jit(solution)/shard_map/all_to_all | solution.py:30
  109.9 0.4 copy.31
  110.3 0.7 reshape.85
  111.2 14.7 %all_gather.9 = bf16[128,2048]{1,0:T(8,128)(2,1)S(1)} all-gather(bf16[16,2048]{1,0:T(8,128)(2,1)S(1)} %fusion.26), channel_id=1, replica_groups=mesh['zh'=4,'zl'=2,'yh'=4,'yl'=2,'x'=4,'c'=2] {'x','c'}, dimensions={0}, use_global_device_ids=true | all-gather | bytes 589824 | tf_op jit(solution)/shard_map/all_gather | solution.py:204
  125.9 2.5 %fusion.3 = bf16[128,768]{1,0:T(8,128)(2,1)S(1)} fusion(bf16[128,2048]{1,0:T(8,128)(2,1)S(1)} %all_gather.9, bf16[2048,1152]{1,0:T(8,128)(2,1)} %all-gather.2.cloned.1.call-done), kind=kOutput, calls=%fused_computation.7 | convolution fusion | flops 402751488 | bytes 3866624 | tf_op jit(solution)/shard_map/dot_general | solution.py:99
  128.4 2.1 %convolution_convert_fusion = bf16[128,2048]{1,0:T(8,128)(2,1)S(1)} fusion(bf16[2048,1152]{1,0:T(8,128)(2,1)} %all-gather.2.cloned.1.call-done, f32[128,384]{1,0:T(8,128)S(1)} %get-tuple-element.28, f32[128,384]{1,0:T(8,128)S(1)} %get-tuple-element.27, f32[384]{0:T(512)S(1)} %get-tuple-element.13, f32[384]{0:T(512)S(1)} %get-tuple-element.14, ...), kind=kOutput, calls=%fused_computation.2 | convolution fusion | flops 202375168 | bytes 2499584 | tf_op jit(solution)/shard_map/dot_general | solution.py:211
  130.5 12.0 %all_to_all.25 = bf16[8,16,2048]{2,1,0:T(8,128)(2,1)S(1)} all-to-all(bf16[8,16,2048]{2,1,0:T(8,128)(2,1)S(1)} %bitcast.48), channel_id=1, replica_groups=mesh['zh'=4,'zl'=2,'yh'=4,'yl'=2,'x'=4,'c'=2] {'x','c'}, dimensions={0} | all-to-all | bytes 1048576 | tf_op jit(solution)/shard_map/all_to_all | solution.py:30
  142.6 14.0 %all_gather.11 = bf16[128,2048]{1,0:T(8,128)(2,1)S(1)} all-gather(bf16[16,2048]{1,0:T(8,128)(2,1)S(1)} %fusion.27), channel_id=1, replica_groups=mesh['zh'=4,'zl'=2,'yh'=4,'yl'=2,'x'=4,'c'=2] {'x','c'}, dimensions={0}, use_global_device_ids=true | all-gather | bytes 589824 | tf_op jit(solution)/shard_map/all_gather | solution.py:217
  156.6 0.8 copy.37
  (53 shorter events, 2.9 us)
Async XLA Ops:
  6.5 18.4 %copy-start = (bf16[128,2048]{1,0:T(8,128)(2,1)S(1)}, bf16[128,2048]{1,0:T(8,128)(2,1)}, u32[]{:S(2)}) copy-start(bf16[128,2048]{1,0:T(8,128)(2,1)} %param.14) | copy-start | bytes 1572868
  6.5 119.4 %all-gather.2.cloned.1.call-start = ((), (), s32[]{:S(2)}) async-start(), calls=%async_computation.5 | async-start | bytes 4792320 | tf_op jit(solution)/shard_map/all_gather | solution.py:144
  8.6 16.8 %copy-start.1 = (f32[2048]{0:T(1024)S(1)}, f32[2048]{0:T(1024)}, u32[]{:S(2)}) copy-start(f32[2048]{0:T(1024)} %param.15) | copy-start | bytes 24580
  8.6 50.9 %all-to-all-start = ((bf16[16,32,1024]{2,1,0:T(8,128)(2,1)}), bf16[16,32,1024]{2,1,0:T(8,128)(2,1)S(1)}, u32[]{:S(2)}, u32[]{:S(2)}) async-start(bf16[16,32,1024]{2,1,0:T(8,128)(2,1)} %get-tuple-element.7), calls=%async_computation | async-start | bytes 2097152 | tf_op jit(solution)/shard_map/all_to_all | solution.py:30
  26.0 23.3 %collective-permute-start = (bf16[1,128,512]{1,2,0:T(8,128)(2,1)S(1)}, bf16[1,128,512]{1,2,0:T(8,128)(2,1)S(1)}, u32[]{:S(2)}, u32[]{:S(2)}) collective-permute-start(bf16[1,128,512]{1,2,0:T(8,128)(2,1)S(1)} %get-tuple-element.21), channel_id=1, source_target_pairs={{0,8},{8,0},{64,72},{72,64},{1,9},{9,1},{65,73},{73,65},{2,10},{10... | collective-permute-start | bytes 393224 | tf_op jit(solution)/shard_map/ppermute | solution.py:155
  28.3 21.1 %collective-permute-start.1 = (bf16[1,128,512]{1,2,0:T(8,128)(2,1)S(1)}, bf16[1,128,512]{1,2,0:T(8,128)(2,1)S(1)}, u32[]{:S(2)}, u32[]{:S(2)}) collective-permute-start(bf16[1,128,512]{1,2,0:T(8,128)(2,1)S(1)} %get-tuple-element.20), channel_id=1, source_target_pairs={{0,64},{8,72},{64,0},{72,8},{1,65},{9,73},{65,1},{73,9},{2,66},{10... | collective-permute-start | bytes 393224 | tf_op jit(solution)/shard_map/ppermute | solution.py:155
  31.4 27.3 %collective-permute-start.2 = (bf16[1,128,512]{1,2,0:T(8,128)(2,1)S(1)}, bf16[1,128,512]{1,2,0:T(8,128)(2,1)S(1)}, u32[]{:S(2)}, u32[]{:S(2)}) collective-permute-start(bf16[1,128,512]{1,2,0:T(8,128)(2,1)S(1)} %get-tuple-element.19), channel_id=1, source_target_pairs={{0,72},{8,64},{64,8},{72,0},{1,73},{9,65},{65,9},{73,1},{2,74},{10... | collective-permute-start | bytes 393224 | tf_op jit(solution)/shard_map/ppermute | solution.py:155
  61.4 15.1 %all-to-all-start.1 = ((bf16[4,144,768]{2,1,0:T(8,128)(2,1)}), bf16[4,144,768]{2,1,0:T(8,128)(2,1)S(1)}, u32[]{:S(2)}, u32[]{:S(2)}) async-start(bf16[4,144,768]{2,1,0:T(8,128)(2,1)} %maximum_maximum_fusion), calls=%async_computation.1 | async-start | bytes 1769472 | tf_op jit(solution)/shard_map/all_to_all | solution.py:30
  76.7 1.2 copy-start.5
  78.7 20.0 %copy-start.3 = (f32[3,384]{1,0:T(4,128)S(1)}, f32[3,384]{1,0:T(4,128)}, u32[]{:S(2)}) copy-start(f32[3,384]{1,0:T(4,128)} %param.26) | copy-start | bytes 13828
  78.7 20.0 %copy-start.4 = (f32[3,384]{1,0:T(4,128)S(1)}, f32[3,384]{1,0:T(4,128)}, u32[]{:S(2)}) copy-start(f32[3,384]{1,0:T(4,128)} %param.25) | copy-start | bytes 13828
  78.7 7.7 %all-to-all-start.2 = ((bf16[4,128,256]{2,1,0:T(8,128)(2,1)}), bf16[4,128,256]{2,1,0:T(8,128)(2,1)S(1)}, u32[]{:S(2)}, u32[]{:S(2)}) async-start(bf16[4,128,256]{2,1,0:T(8,128)(2,1)} %broadcast_in_dim.9), calls=%async_computation.2 | async-start | bytes 524288 | tf_op jit(solution)/shard_map/all_to_all | solution.py:30
  86.8 6.1 %collective-permute-start.3 = (bf16[16,16,512]{2,1,0:T(8,128)(2,1)S(1)}, bf16[16,16,512]{2,1,0:T(8,128)(2,1)S(1)}, u32[]{:S(2)}, u32[]{:S(2)}) collective-permute-start(bf16[16,16,512]{2,1,0:T(8,128)(2,1)S(1)} %dynamic-slice_bitcast_fusion), channel_id=1, source_target_pairs={{0,1},{1,0},{2,3},{3,2},{4,5},{5,4},{6,7},{7,6},{8,9},{9,8},{10,11... | collective-permute-start | bytes 786440 | tf_op jit(solution)/shard_map/ppermute | solution.py:199
  93.7 17.5 %copy-start.2 = (f32[2048]{0:T(1024)S(1)}, f32[2048]{0:T(1024)}, u32[]{:S(2)}) copy-start(f32[2048]{0:T(1024)} %param.22) | copy-start | bytes 24580
  93.7 15.9 %all-to-all-start.3 = ((bf16[16,16,512]{2,1,0:T(8,128)(2,1)}), bf16[16,16,512]{2,1,0:T(8,128)(2,1)S(1)}, u32[]{:S(2)}, u32[]{:S(2)}) async-start(bf16[16,16,512]{2,1,0:T(8,128)(2,1)} %fusion.10), calls=%async_computation.3 | async-start | bytes 524288 | tf_op jit(solution)/shard_map/all_to_all | solution.py:30
Sparse Core Ops, SparseCore 0:
  10.3 108.4 all-gather.1
